TPU v7x, 32 devices: a whole 2x2x4 slice. The times are simulated.
32 devices in a mesh: sp: 8 (over z, x), tp: 4 (over y, core).
Axes of the slice: x: 2, y: 2, z: 4, core: 2. Of those that a mesh axis runs over, the one named last changes fastest.
Arguments:
- queries: bfloat16 [1024, 2048], P('sp', 'tp'), may hold values from -440 to 440
- key_rows: bfloat16 [1024, 1024], P('sp', 'tp'), may hold values from -6 to 6
- value_rows: bfloat16 [1024, 1024], P('sp', 'tp'), may hold values from -6 to 6
- sink_logits: float32 [32], P('tp'), may hold values from -6 to 6
- out_weight: bfloat16 [2048, 2048], P('tp'), may hold values from -0.125 to 0.125
- residual: bfloat16 [1024, 2048], P('sp'), may hold values from -3 to 3
- norm_gain: float32 [2048], replicated, may hold values from 0.1 to 1.9
- routes: int32 [1024, 2], P('sp'), may hold values from 0 to 7, all different within a row; in each aligned block of 128 rows (0 to 127, 128 to 255, ...) at most 64 rows name the same one
- route_weights: float32 [1024, 2], P('sp'), may hold values from 0.2 to 1
- gate_weight: bfloat16 [8, 2048, 4096], P('sp', None, 'tp'), may hold values from -0.125 to 0.125
- up_weight: bfloat16 [8, 2048, 4096], P('sp', None, 'tp'), may hold values from -0.125 to 0.125
- down_weight: bfloat16 [8, 4096, 2048], P('sp', 'tp'), may hold values from -0.09375 to 0.09375
Outputs:
- layer_out: bfloat16 [1024, 2048], P('sp')
Inputs may be any that keep to these rules, and one draw needn't show every extreme that they name: `routes`: each row names 2 different experts. In each aligned block of 128 rows (the rows of one index of sp) no expert is named by more than 64 rows, a bound that some block reaches.
All inputs are finite; a program needn't handle non-finite values.
Results may differ from a plain program's by a relative error of at most 0.02.
Values may be sent and summed in bfloat16 or wider, within the bound.
A program may use at most 64 MiB of HBM per device.

v0:
```python
import jax
import jax.numpy as jnp
from jax import lax
from jax.sharding import PartitionSpec as P

HEAD_DIM = 64
QH = 32
WINDOW = 128
TOP = 2


def from_behind(array, axis, by):
    peers = lax.axis_size(axis)
    pairs = [(i, i + by) for i in range(peers) if 0 <= i + by < peers]
    return lax.ppermute(array, axis, pairs)


def per_device(
    queries,
    key_rows,
    value_rows,
    sink_logits,
    out_weight,
    residual,
    norm_gain,
    routes,
    route_weights,
    gate_weight,
    up_weight,
    down_weight,
):
    rows_here = queries.shape[0]
    width = residual.shape[1]
    heads_here = queries.shape[1] // HEAD_DIM
    kv_here = key_rows.shape[1] // HEAD_DIM
    group_size = heads_here // kv_here
    blocks = rows_here // WINDOW
    rim_rows = jnp.stack([key_rows, value_rows])
    before = from_behind(rim_rows, "sp", 1)
    key_ext = jnp.concatenate([before[0], key_rows], axis=0).reshape(
        blocks + 1, WINDOW, kv_here, HEAD_DIM
    )
    val_ext = jnp.concatenate([before[1], value_rows], axis=0).reshape(
        blocks + 1, WINDOW, kv_here, HEAD_DIM
    )
    key_pair = jnp.concatenate([key_ext[:-1], key_ext[1:]], axis=1)
    val_pair = jnp.concatenate([val_ext[:-1], val_ext[1:]], axis=1)
    query_blocks = queries.reshape(blocks, WINDOW, kv_here, group_size, HEAD_DIM)
    scores = jnp.einsum(
        "bqkgd,bckd->bkgqc", query_blocks, key_pair, preferred_element_type=jnp.float32
    ) * HEAD_DIM ** (-0.5)
    distance = jnp.arange(WINDOW)[:, None] + WINDOW - jnp.arange(2 * WINDOW)[None, :]
    offset = lax.axis_index("sp") * rows_here
    key_global = (
        offset
        + jnp.arange(blocks)[:, None, None] * WINDOW
        + jnp.arange(2 * WINDOW)[None, None, :]
        - WINDOW
    )
    allowed = (distance >= 0)[None] & (distance <= WINDOW)[None] & (key_global >= 0)
    head_ids = lax.axis_index("tp") * heads_here + jnp.arange(heads_here)
    slopes = jnp.exp2(-8.0 * (head_ids + 1).astype(jnp.float32) / QH).reshape(kv_here, group_size)
    scores = scores - slopes[None, :, :, None, None] * distance.astype(jnp.float32)
    scores = jnp.where(allowed[:, None, None], scores, -jnp.inf)
    row_peak = jnp.max(scores, axis=-1, keepdims=True)
    log_total = row_peak + jnp.log(jnp.sum(jnp.exp(scores - row_peak), axis=-1, keepdims=True))
    weights_bf = jnp.exp(scores - log_total).astype(jnp.bfloat16)
    attended = jnp.einsum(
        "bkgqc,bckd->bqkgd", weights_bf, val_pair, preferred_element_type=jnp.float32
    )
    keep_factor = jax.nn.sigmoid(
        log_total[..., 0] - sink_logits.reshape(kv_here, group_size)[None, :, :, None]
    )
    keep_factor = jnp.transpose(keep_factor, (0, 3, 1, 2))[..., None]
    attended = (
        (attended * keep_factor).astype(jnp.bfloat16).reshape(rows_here, heads_here * HEAD_DIM)
    )
    partial_value = jnp.dot(attended, out_weight, preferred_element_type=jnp.float32)
    partial_value = lax.optimization_barrier(partial_value.astype(jnp.bfloat16)).astype(jnp.float32)
    head_total = lax.psum(partial_value.astype(jnp.bfloat16), "tp").astype(jnp.float32)
    mixed_state = (residual.astype(jnp.float32) + head_total).astype(jnp.bfloat16)
    state32 = mixed_state.astype(jnp.float32)
    normed = (
        state32 * lax.rsqrt(jnp.mean(state32 * state32, axis=-1, keepdims=True) + 1e-06) * norm_gain
    ).astype(jnp.bfloat16)
    experts = lax.axis_size("sp")
    capacity = 2 * rows_here * TOP // experts
    flat_routes = routes.reshape(-1)
    member = (flat_routes[:, None] == jnp.arange(experts)[None, :]).astype(jnp.int32)
    slot_rank = jnp.sum((jnp.cumsum(member, axis=0) - 1) * member, axis=1)
    slot_index = flat_routes * capacity + slot_rank
    picker = (jnp.arange(experts * capacity)[:, None] == slot_index[None, :]).astype(jnp.int32)
    picker = jnp.sum(picker.reshape(experts * capacity, rows_here, TOP), axis=-1).astype(
        jnp.bfloat16
    )
    outgoing = (
        jnp.dot(picker, normed, preferred_element_type=jnp.float32)
        .astype(jnp.bfloat16)
        .reshape(experts, capacity, width)
    )
    w_gate = gate_weight[0]
    w_up = up_weight[0]
    w_down = down_weight[0]
    slot_share = capacity // lax.axis_size("tp")
    mine = lax.dynamic_slice_in_dim(outgoing, lax.axis_index("tp") * slot_share, slot_share, 1)
    arrived = lax.all_to_all(mine, "sp", split_axis=0, concat_axis=0, tiled=True)
    gathered = lax.all_gather(arrived, "tp", axis=1, tiled=True)
    flat_rows = gathered.reshape(-1, width)
    gate_pre = jnp.dot(flat_rows, w_gate, preferred_element_type=jnp.float32)
    up_pre = jnp.dot(flat_rows, w_up, preferred_element_type=jnp.float32)
    activated = (jax.nn.silu(gate_pre) * up_pre).astype(jnp.bfloat16)
    result = jnp.dot(activated, w_down, preferred_element_type=jnp.float32)
    result = lax.optimization_barrier(result.astype(jnp.bfloat16)).astype(jnp.float32)
    summed = lax.psum_scatter(
        result.reshape(gathered.shape).astype(jnp.bfloat16), "tp", scatter_dimension=1, tiled=True
    )
    back_rows = lax.all_to_all(summed, "sp", split_axis=0, concat_axis=0, tiled=True)
    returned = lax.all_gather(back_rows, "tp", axis=1, tiled=True)
    slot_table = returned.reshape(experts * capacity, width)
    picked = jnp.take(slot_table, slot_index, axis=0).reshape(rows_here, TOP, width)
    expert_mix = jnp.sum(route_weights[..., None] * picked.astype(jnp.float32), axis=1)
    return (state32 + expert_mix).astype(jnp.bfloat16)


def solution(mesh):
    placed = (
        P("sp", "tp"),
        P("sp", "tp"),
        P("sp", "tp"),
        P("tp"),
        P("tp", None),
        P("sp", None),
        P(),
        P("sp", None),
        P("sp", None),
        P("sp", None, "tp"),
        P("sp", None, "tp"),
        P("sp", "tp", None),
    )
    return jax.shard_map(
        per_device, mesh=mesh, in_specs=placed, out_specs=P("sp", None), check_vma=False
    )
```

profile of v0, /device:TPU:0, one launch (start us, length us, event | category | flops | bytes accessed | tf_op | source)
XLA Modules:
  0.0 208.5 jit_solution(12147156466361507940)
XLA Ops:
  6.5 1.0 pad_maximum_fusion
  7.6 4.9 %collective-permute-start = (bf16[2,128,256]{2,1,0:T(8,128)(2,1)S(1)}, bf16[2,128,256]{2,1,0:T(8,128)(2,1)S(1)}, u32[]{:S(2)}, u32[]{:S(2)}) collective-permute-start(bf16[2,128,256]{2,1,0:T(8,128)(2,1)S(1)} %pad_maximum_fusion), channel_id=1, source_target_pairs={{0,4},{4,8},{8,12},{12,16},{16,20},{20,24},{24,28},{1,5},{5,9},{9,... | collective-permute-start | bytes 393224 | tf_op jit(solution)/shard_map/ppermute | solution.py:15
  12.5 0.8 copy.50
  13.3 0.1 eq.40
  13.4 0.1 reshape.307
  13.6 0.1 fusion.37
  13.7 0.6 reduce-window.6
  14.3 0.2 slice_reduce_fusion
  14.6 0.1 fusion.38
  14.6 1.0 copy.46
  15.6 1.0 copy.44
  16.6 1.0 copy.47
  17.6 0.7 sub.85
  18.3 0.1 reduce_sum.51
  18.5 0.1 copy.52
  18.6 0.1 copy.45
  18.7 0.1 copy.43
  18.8 0.4 fusion.51
  19.3 0.2 exponential_reduce_fusion
  19.4 0.1 fusion.44
  19.5 0.3 fusion.15
  19.9 1.3 convolution_convert_fusion.1
  21.1 0.0 all-reduce.2.cloned.1.call-update
  21.2 0.0 all-gather.3.cloned.1.call-start
  21.2 0.1 convert_reduce_fusion
  21.3 33.7 %all-reduce.2.cloned.1.call-done = bf16[128,2048]{1,0:T(8,128)(2,1)} async-done(((bf16[128,2048]{1,0:T(8,128)(2,1)}), bf16[128,2048]{1,0:T(8,128)(2,1)}) %all-reduce.2.cloned.1.call-update) | async-done | bytes 524304 | tf_op jit(solution)/shard_map/psum | solution.py:80
  55.0 1.3 fusion.16
  56.3 1.8 convolution_convert_fusion
  58.2 18.9 %all_to_all.10 = bf16[8,16,2048]{2,1,0:T(8,128)(2,1)} all-to-all(bf16[8,16,2048]{2,1,0:T(8,128)(2,1)S(1)} %constant_dynamic-slice_fusion), channel_id=1, replica_groups=mesh['sp'=8,'tp'=4] {'sp'}, dimensions={0} | all-to-all | bytes 1048576 | tf_op jit(solution)/shard_map/all_to_all | solution.py:106
  77.2 0.0 all-gather.3.cloned.1.call-update
  77.2 0.0 reduce-scatter.2.cloned.1.call-start
  77.2 21.3 %all-gather.3.cloned.1.call-done = bf16[8,64,2048]{2,1,0:T(8,128)(2,1)} async-done(((bf16[8,16,2048]{2,1,0:T(8,128)(2,1)}), bf16[8,64,2048]{2,1,0:T(8,128)(2,1)}) %all-gather.3.cloned.1.call-update) | async-done | bytes 2097168 | tf_op jit(solution)/shard_map/all_gather | solution.py:107
  98.5 6.5 %fusion.4 = f32[512,1024]{1,0:T(8,128)} fusion(bf16[512,2048]{1,0:T(8,128)(2,1)} %bitcast.102, bf16[1,2048,1024]{2,1,0:T(8,128)(2,1)} %param.21), kind=kOutput, calls=%fused_computation.5 | convolution fusion | flops 2147483648 | bytes 8388608 | tf_op jit(solution)/shard_map/dot_general | solution.py:109
  105.0 10.5 %fusion.6 = bf16[512,2048]{1,0:T(8,128)(2,1)} fusion(bf16[1,1024,2048]{2,1,0:T(8,128)(2,1)} %param.23, f32[512,1024]{1,0:T(8,128)} %fusion.4, bf16[512,2048]{1,0:T(8,128)(2,1)} %bitcast.103, bf16[1,2048,1024]{2,1,0:T(8,128)(2,1)} %param.22), kind=kOutput, calls=%fused_computation.7 | convolution fusion | flops 4299161600 | bytes 14680064 | tf_op jit(solution)/shard_map/dot_general | solution.py:112
  115.5 0.0 reduce-scatter.2.cloned.1.call-update
  115.5 0.0 all-gather.5.cloned.1.call-start
  115.6 31.3 %reduce-scatter.2.cloned.1.call-done = bf16[8,16,2048]{2,1,0:T(8,128)(2,1)} async-done(((bf16[8,64,2048]{2,1,0:T(8,128)(2,1)}), bf16[8,16,2048]{2,1,0:T(8,128)(2,1)}) %reduce-scatter.2.cloned.1.call-update) | async-done | bytes 524304 | tf_op jit(solution)/shard_map/reduce_scatter | solution.py:114
  146.9 20.0 %all_to_all.11 = bf16[8,16,2048]{2,1,0:T(8,128)(2,1)} all-to-all(bf16[8,16,2048]{2,1,0:T(8,128)(2,1)} %reduce-scatter.2.cloned.1.call-done), channel_id=1, replica_groups=mesh['sp'=8,'tp'=4] {'sp'}, dimensions={0} | all-to-all | bytes 1048576 | tf_op jit(solution)/shard_map/all_to_all | solution.py:117
  166.8 0.0 all-gather.5.cloned.1.call-update
  166.9 0.1 copy.54
  167.0 0.1 mul.138
  167.1 0.1 copy.53
  167.3 0.1 copy.49
  167.4 20.3 %all-gather.5.cloned.1.call-done = bf16[8,64,2048]{2,1,0:T(8,128)(2,1)} async-done(((bf16[8,16,2048]{2,1,0:T(8,128)(2,1)}), bf16[8,64,2048]{2,1,0:T(8,128)(2,1)}) %all-gather.5.cloned.1.call-update) | async-done | bytes 2097168 | tf_op jit(solution)/shard_map/all_gather | solution.py:118
  187.7 5.2 %gather_fusion = bf16[256,2048]{1,0:T(8,128)(2,1)} fusion(bf16[512,2048]{1,0:T(8,128)(2,1)} %bitcast.89, s32[1024]{0:T(1024)S(1)} %pad_clamp_fusion), kind=kCustom, calls=%fused_computation | custom fusion | bytes 2098176 | tf_op jit(solution)/shard_map/jit(_take)/gather | solution.py:120
  192.9 2.6 %gather.7 = bf16[128,2,2048]{2,1,0:T(2,128)(2,1)} reshape(bf16[256,2048]{1,0:T(8,128)(2,1)} %gather_fusion) | data formatting | bytes 2097152 | tf_op jit(solution)/shard_map/jit(_take)/gather | solution.py:120
  195.5 5.5 %multiply_reduce_fusion = f32[128,2048]{1,0:T(8,128)S(1)} fusion(bf16[128,2,2048]{2,1,0:T(2,128)(2,1)} %gather.7, pred[128,2]{1,0:T(8,128)(4,1)S(1)} %copy.53, f32[128,2]{1,0:T(8,128)S(1)} %copy.49), kind=kLoop, calls=%fused_computation.10 | loop fusion | flops 1835008 | bytes 2098432 | tf_op jit(solution)/shard_map/reduce_sum | solution.py:121
  201.0 1.0 fusion.19
  (28 shorter events, 0.2 us)
Async XLA Ops:
  6.5 13.3 %copy-start = (bf16[512,2048]{1,0:T(8,128)(2,1)S(1)}, bf16[512,2048]{1,0:T(8,128)(2,1)}, u32[]{:S(2)}) copy-start(bf16[512,2048]{1,0:T(8,128)(2,1)} %param.16) | copy-start | bytes 6291460
  6.5 48.5 %all-reduce.2.cloned.1.call-start = ((), (), s32[]{:S(2)}) async-start(), calls=%async_computation.3 | async-start | bytes 1048576 | tf_op jit(solution)/shard_map/psum | solution.py:80
  7.6 11.0 %collective-permute-start = (bf16[2,128,256]{2,1,0:T(8,128)(2,1)S(1)}, bf16[2,128,256]{2,1,0:T(8,128)(2,1)S(1)}, u32[]{:S(2)}, u32[]{:S(2)}) collective-permute-start(bf16[2,128,256]{2,1,0:T(8,128)(2,1)S(1)} %pad_maximum_fusion), channel_id=1, source_target_pairs={{0,4},{4,8},{8,12},{12,16},{16,20},{20,24},{24,28},{1,5},{5,9},{9,... | collective-permute-start | bytes 393224 | tf_op jit(solution)/shard_map/ppermute | solution.py:15
  19.5 1.7 copy-start.3
  19.8 35.2 %copy-start.1 = (bf16[128,2048]{1,0:T(8,128)(2,1)S(1)}, bf16[128,2048]{1,0:T(8,128)(2,1)}, u32[]{:S(2)}) copy-start(bf16[128,2048]{1,0:T(8,128)(2,1)} %param.17) | copy-start | bytes 1572868
  19.8 36.5 %copy-start.4 = (f32[2048]{0:T(1024)S(1)}, f32[2048]{0:T(1024)}, u32[]{:S(2)}) copy-start(f32[2048]{0:T(1024)} %param.18) | copy-start | bytes 24580
  21.2 77.3 %all-gather.3.cloned.1.call-start = ((), (), s32[]{:S(2)}) async-start(), calls=%async_computation.4 | async-start | bytes 2621440 | tf_op jit(solution)/shard_map/all_gather | solution.py:107
  77.2 69.7 %reduce-scatter.2.cloned.1.call-start = ((), (), s32[]{:S(2)}) async-start(), calls=%async_computation.5 | async-start | bytes 2621440 | tf_op jit(solution)/shard_map/reduce_scatter | solution.py:114
  115.5 51.8 %copy-start.5 = (f32[128,2]{0,1:T(2,128)S(1)}, f32[128,2]{0,1:T(2,128)}, u32[]{:S(2)}) copy-start(f32[128,2]{0,1:T(2,128)} %param.20) | copy-start | bytes 3076
  115.5 72.1 %all-gather.5.cloned.1.call-start = ((), (), s32[]{:S(2)}) async-start(), calls=%async_computation.6 | async-start | bytes 2621440 | tf_op jit(solution)/shard_map/all_gather | solution.py:118
  192.9 8.1 %copy-start.2 = (bf16[128,2048]{1,0:T(8,128)(2,1)S(1)}, bf16[128,2048]{1,0:T(8,128)(2,1)}, u32[]{:S(2)}) copy-start(bf16[128,2048]{1,0:T(8,128)(2,1)} %all-reduce.2.cloned.1.call-done) | copy-start | bytes 1572868
Sparse Core Ops, SparseCore 0:
  21.3 33.7 all-reduce.1
  77.3 21.1 all-gather.2
  115.7 31.1 reduce-scatter.1
  167.0 20.6 all-gather.4
where the time goes:
time: 209 us
  waiting for transfers between devices  107 us (51%)
  blocking collectives  38.9 us (19%)
  matrix products  20.8 us (10%)
  local copies, waits for them, and re-layouts  13.8 us (7%)
  between operations  13.4 us (6%)
  other arithmetic  10 us (5%)
  starting transfers between devices  5.01 us (2%)
    psum x1, waiting for transfers between devices, per_device(): lax.psum(partial_value.astype(jnp.bfloat16), 'tp').astype(jnp.float32)  33.7 us
    reduce_scatter x1, waiting for transfers between devices, per_device(): lax.psum_scatter(result.reshape(gathered.shape).astype(jnp.bfloat16), 'tp...  31.3 us
    all_gather x1, waiting for transfers between devices, per_device(): gathered = lax.all_gather(arrived, 'tp', axis=1, tiled=True)  21.3 us
    all_gather x1, waiting for transfers between devices, per_device(): returned = lax.all_gather(back_rows, 'tp', axis=1, tiled=True)  20.3 us
    all_to_all x1, blocking collectives, per_device(): lax.all_to_all(summed, 'sp', split_axis=0, concat_axis=0, tiled=True)  20 us
    all_to_all x1, blocking collectives, per_device(): lax.all_to_all(mine, 'sp', split_axis=0, concat_axis=0, tiled=True)  18.9 us
    dot_general x1, matrix products, per_device(): result = jnp.dot(activated, w_down, preferred_element_type=jnp.float32)  10.5 us
    gather x2, local copies, waits for them, and re-layouts, per_device(): jnp.take(slot_table, slot_index, axis=0).reshape(rows_here, TOP, width)  7.81 us
  transfers between devices with their start and end apart: 5, of which 4 were waited for; matrix products, arithmetic and copies ran while one was open for 3% of the time, Pallas kernels for 0%

commit v1 on v0

--- a/solution.py
+++ b/solution.py
@@ -77,7 +77,9 @@
     )
     partial_value = jnp.dot(attended, out_weight, preferred_element_type=jnp.float32)
     partial_value = lax.optimization_barrier(partial_value.astype(jnp.bfloat16)).astype(jnp.float32)
-    head_total = lax.psum(partial_value.astype(jnp.bfloat16), "tp").astype(jnp.float32)
+    head_total = (
+        jax.lax.all_gather(partial_value.astype(jnp.bfloat16), "tp").sum(axis=0).astype(jnp.float32)
+    )
     mixed_state = (residual.astype(jnp.float32) + head_total).astype(jnp.bfloat16)
     state32 = mixed_state.astype(jnp.float32)
     normed = (

time: 209 us -> 197 us (0.943)
  waiting for transfers between devices: 107 us -> 94.5 us
    psum x1 -> x0, waiting for transfers between devices: 33.7 us -> none  [per_device(): lax.psum(partial_value.astype(jnp.bfloat16), 'tp').astype(jnp.float32)]
    all_gather x0 -> x1, waiting for transfers between devices: none -> 22.1 us  [per_device(): jax.lax.all_gather(partial_value.astype(jnp.bfloat16), 'tp').sum(axis=0)]
where the time goes in v1:
time: 197 us
  waiting for transfers between devices  94.5 us (48%)
  blocking collectives  40.3 us (20%)
  matrix products  19.8 us (10%)
  between operations  13.4 us (7%)
  local copies, waits for them, and re-layouts  13 us (7%)
  other arithmetic  11 us (6%)
  starting transfers between devices  5.01 us (3%)
    reduce_scatter x1, waiting for transfers between devices, per_device(): lax.psum_scatter(result.reshape(gathered.shape).astype(jnp.bfloat16), 'tp...  31.3 us
    all_gather x1, waiting for transfers between devices, per_device(): jax.lax.all_gather(partial_value.astype(jnp.bfloat16), 'tp').sum(axis=0)  22.1 us
    all_gather x1, waiting for transfers between devices, per_device(): gathered = lax.all_gather(arrived, 'tp', axis=1, tiled=True)  20.8 us
    all_to_all x1, blocking collectives, per_device(): lax.all_to_all(mine, 'sp', split_axis=0, concat_axis=0, tiled=True)  20.3 us
    all_gather x1, waiting for transfers between devices, per_device(): returned = lax.all_gather(back_rows, 'tp', axis=1, tiled=True)  20.3 us
    all_to_all x1, blocking collectives, per_device(): lax.all_to_all(summed, 'sp', split_axis=0, concat_axis=0, tiled=True)  20 us
    dot_general x1, matrix products, per_device(): result = jnp.dot(activated, w_down, preferred_element_type=jnp.float32)  10.5 us
    gather x2, local copies, waits for them, and re-layouts, per_device(): jnp.take(slot_table, slot_index, axis=0).reshape(rows_here, TOP, width)  7.75 us
  transfers between devices with their start and end apart: 5, of which 4 were waited for; matrix products, arithmetic and copies ran while one was open for 3% of the time, Pallas kernels for 0%

profile of v1, /device:TPU:0, one launch (start us, length us, event | category | flops | bytes accessed | tf_op | source)
XLA Modules:
  0.0 197.0 jit_solution(14990933014268275141)
XLA Ops:
  6.5 1.0 pad_maximum_fusion
  7.6 4.9 %collective-permute-start = (bf16[2,128,256]{2,1,0:T(8,128)(2,1)S(1)}, bf16[2,128,256]{2,1,0:T(8,128)(2,1)S(1)}, u32[]{:S(2)}, u32[]{:S(2)}) collective-permute-start(bf16[2,128,256]{2,1,0:T(8,128)(2,1)S(1)} %pad_maximum_fusion), channel_id=1, source_target_pairs={{0,4},{4,8},{8,12},{12,16},{16,20},{20,24},{24,28},{1,5},{5,9},{9,... | collective-permute-start | bytes 393224 | tf_op jit(solution)/shard_map/ppermute | solution.py:15
  12.5 0.1 fusion.37
  12.6 1.0 copy.46
  13.6 1.0 copy.44
  14.5 1.0 copy.47
  15.6 0.7 sub.85
  16.4 0.1 copy.45
  16.5 0.1 copy.43
  16.6 0.4 fusion.51
  17.0 0.2 exponential_reduce_fusion
  17.2 0.1 fusion.44
  17.3 0.3 fusion.15
  17.6 1.3 convolution_convert_fusion.1
  18.9 0.0 all-gather.9.cloned.1.call-update
  18.9 0.0 all-gather.5.cloned.1.call-start
  18.9 0.1 copy.50
  19.1 0.1 eq.40
  19.2 0.1 reshape.307
  19.4 0.6 reduce-window.6
  20.0 0.2 slice_reduce_fusion
  20.2 0.1 fusion.38
  20.3 0.1 reduce_sum.64
  20.5 0.1 copy.52
  20.5 0.1 convert_reduce_fusion
  20.6 22.1 %all-gather.9.cloned.1.call-done = bf16[512,2048]{1,0:T(8,128)(2,1)} async-done(((bf16[128,2048]{1,0:T(8,128)(2,1)}), bf16[512,2048]{1,0:T(8,128)(2,1)}) %all-gather.9.cloned.1.call-update) | async-done | bytes 2097168 | tf_op jit(solution)/shard_map/all_gather | solution.py:81
  42.7 2.0 %reduce_sum.62 = bf16[128,2048]{1,0:T(8,128)(2,1)S(1)} reduce(bf16[4,128,2048]{2,1,0:T(8,128)(2,1)} %bitcast.92, bf16[]{:T(256)} %constant.68.clone.1), dimensions={0}, to_apply=%region_2.3 | reduce | flops 786432 | bytes 2621442 | tf_op jit(solution)/shard_map/reduce_sum | solution.py:81
  44.8 0.3 fusion.16
  45.0 0.8 convolution_convert_fusion
  45.9 20.3 %all_to_all.10 = bf16[8,16,2048]{2,1,0:T(8,128)(2,1)} all-to-all(bf16[8,16,2048]{2,1,0:T(8,128)(2,1)S(1)} %constant_dynamic-slice_fusion), channel_id=1, replica_groups=mesh['sp'=8,'tp'=4] {'sp'}, dimensions={0} | all-to-all | bytes 1048576 | tf_op jit(solution)/shard_map/all_to_all | solution.py:108
  66.2 0.0 all-gather.5.cloned.1.call-update
  66.2 0.0 reduce-scatter.2.cloned.1.call-start
  66.2 20.8 %all-gather.5.cloned.1.call-done = bf16[8,64,2048]{2,1,0:T(8,128)(2,1)} async-done(((bf16[8,16,2048]{2,1,0:T(8,128)(2,1)}), bf16[8,64,2048]{2,1,0:T(8,128)(2,1)}) %all-gather.5.cloned.1.call-update) | async-done | bytes 2097168 | tf_op jit(solution)/shard_map/all_gather | solution.py:109
  87.0 6.5 %fusion.4 = f32[512,1024]{1,0:T(8,128)} fusion(bf16[512,2048]{1,0:T(8,128)(2,1)} %bitcast.104, bf16[1,2048,1024]{2,1,0:T(8,128)(2,1)} %param.21), kind=kOutput, calls=%fused_computation.5 | convolution fusion | flops 2147483648 | bytes 8388608 | tf_op jit(solution)/shard_map/dot_general | solution.py:111
  93.5 10.5 %fusion.6 = bf16[512,2048]{1,0:T(8,128)(2,1)} fusion(bf16[1,1024,2048]{2,1,0:T(8,128)(2,1)} %param.23, f32[512,1024]{1,0:T(8,128)} %fusion.4, bf16[512,2048]{1,0:T(8,128)(2,1)} %bitcast.105, bf16[1,2048,1024]{2,1,0:T(8,128)(2,1)} %param.22), kind=kOutput, calls=%fused_computation.7 | convolution fusion | flops 4299161600 | bytes 14680064 | tf_op jit(solution)/shard_map/dot_general | solution.py:114
  104.1 0.0 all-gather.7.cloned.1.call-start
  104.1 31.3 %reduce-scatter.2.cloned.1.call-done = bf16[8,16,2048]{2,1,0:T(8,128)(2,1)} async-done(((bf16[8,64,2048]{2,1,0:T(8,128)(2,1)}), bf16[8,16,2048]{2,1,0:T(8,128)(2,1)}) %reduce-scatter.2.cloned.1.call-update) | async-done | bytes 524304 | tf_op jit(solution)/shard_map/reduce_scatter | solution.py:116
  135.4 20.0 %all_to_all.11 = bf16[8,16,2048]{2,1,0:T(8,128)(2,1)} all-to-all(bf16[8,16,2048]{2,1,0:T(8,128)(2,1)} %reduce-scatter.2.cloned.1.call-done), channel_id=1, replica_groups=mesh['sp'=8,'tp'=4] {'sp'}, dimensions={0} | all-to-all | bytes 1048576 | tf_op jit(solution)/shard_map/all_to_all | solution.py:119
  155.4 0.0 all-gather.7.cloned.1.call-update
  155.4 0.1 copy.54
  155.5 0.1 mul.138
  155.7 0.1 copy.53
  155.8 0.1 copy.49
  155.9 20.3 %all-gather.7.cloned.1.call-done = bf16[8,64,2048]{2,1,0:T(8,128)(2,1)} async-done(((bf16[8,16,2048]{2,1,0:T(8,128)(2,1)}), bf16[8,64,2048]{2,1,0:T(8,128)(2,1)}) %all-gather.7.cloned.1.call-update) | async-done | bytes 2097168 | tf_op jit(solution)/shard_map/all_gather | solution.py:120
  176.2 5.2 %gather_fusion = bf16[256,2048]{1,0:T(8,128)(2,1)} fusion(bf16[512,2048]{1,0:T(8,128)(2,1)} %bitcast.90, s32[1024]{0:T(1024)S(1)} %pad_clamp_fusion), kind=kCustom, calls=%fused_computation | custom fusion | bytes 2098176 | tf_op jit(solution)/shard_map/jit(_take)/gather | solution.py:122
  181.4 2.5 %gather.7 = bf16[128,2,2048]{2,1,0:T(2,128)(2,1)} reshape(bf16[256,2048]{1,0:T(8,128)(2,1)} %gather_fusion) | data formatting | bytes 2097152 | tf_op jit(solution)/shard_map/jit(_take)/gather | solution.py:122
  184.0 5.5 %multiply_reduce_fusion = f32[128,2048]{1,0:T(8,128)S(1)} fusion(bf16[128,2,2048]{2,1,0:T(2,128)(2,1)} %gather.7, pred[128,2]{1,0:T(8,128)(4,1)S(1)} %copy.53, f32[128,2]{1,0:T(8,128)S(1)} %copy.49), kind=kLoop, calls=%fused_computation.10 | loop fusion | flops 1835008 | bytes 2098432 | tf_op jit(solution)/shard_map/reduce_sum | solution.py:123
  189.4 1.0 fusion.19
  (27 shorter events, 0.2 us)
Async XLA Ops:
  6.5 11.0 %copy-start = (bf16[512,2048]{1,0:T(8,128)(2,1)S(1)}, bf16[512,2048]{1,0:T(8,128)(2,1)}, u32[]{:S(2)}) copy-start(bf16[512,2048]{1,0:T(8,128)(2,1)} %param.16) | copy-start | bytes 6291460
  6.5 36.2 %all-gather.9.cloned.1.call-start = ((), (), s32[]{:S(2)}) async-start(), calls=%async_computation.6 | async-start | bytes 2621440 | tf_op jit(solution)/shard_map/all_gather | solution.py:81
  7.6 8.8 %collective-permute-start = (bf16[2,128,256]{2,1,0:T(8,128)(2,1)S(1)}, bf16[2,128,256]{2,1,0:T(8,128)(2,1)S(1)}, u32[]{:S(2)}, u32[]{:S(2)}) collective-permute-start(bf16[2,128,256]{2,1,0:T(8,128)(2,1)S(1)} %pad_maximum_fusion), channel_id=1, source_target_pairs={{0,4},{4,8},{8,12},{12,16},{16,20},{20,24},{24,28},{1,5},{5,9},{9,... | collective-permute-start | bytes 393224 | tf_op jit(solution)/shard_map/ppermute | solution.py:15
  17.3 1.7 copy-start.2
  18.9 25.9 %copy-start.1 = (bf16[128,2048]{1,0:T(8,128)(2,1)S(1)}, bf16[128,2048]{1,0:T(8,128)(2,1)}, u32[]{:S(2)}) copy-start(bf16[128,2048]{1,0:T(8,128)(2,1)} %param.17) | copy-start | bytes 1572868
  18.9 68.1 %all-gather.5.cloned.1.call-start = ((), (), s32[]{:S(2)}) async-start(), calls=%async_computation.3 | async-start | bytes 2621440 | tf_op jit(solution)/shard_map/all_gather | solution.py:109
  19.2 25.8 %copy-start.3 = (f32[2048]{0:T(1024)S(1)}, f32[2048]{0:T(1024)}, u32[]{:S(2)}) copy-start(f32[2048]{0:T(1024)} %param.18) | copy-start | bytes 24580
  66.2 69.2 %reduce-scatter.2.cloned.1.call-start = ((), (), s32[]{:S(2)}) async-start(), calls=%async_computation.4 | async-start | bytes 2621440 | tf_op jit(solution)/shard_map/reduce_scatter | solution.py:116
  104.0 51.8 %copy-start.4 = (f32[128,2]{0,1:T(2,128)S(1)}, f32[128,2]{0,1:T(2,128)}, u32[]{:S(2)}) copy-start(f32[128,2]{0,1:T(2,128)} %param.20) | copy-start | bytes 3076
  104.1 72.1 %all-gather.7.cloned.1.call-start = ((), (), s32[]{:S(2)}) async-start(), calls=%async_computation.5 | async-start | bytes 2621440 | tf_op jit(solution)/shard_map/all_gather | solution.py:120
Sparse Core Ops, SparseCore 0:
  19.0 23.6 all-gather.8
  66.3 20.6 all-gather.4
  104.2 31.1 reduce-scatter.1
  155.5 20.6 all-gather.6
